TPU v7x, 32 devices: a whole 2x2x4 slice. The times are simulated.
32 devices in a mesh: sp: 8 (over z, y), dp: 4 (over x, core).
Axes of the slice: x: 2, y: 2, z: 4, core: 2. Of those that a mesh axis runs over, the one named last changes fastest.
Arguments:
- query: bfloat16 [4, 1536, 3072], P('dp', 'sp'), may hold values from -18 to 18
- latent: bfloat16 [4, 1536, 1024], P('dp', 'sp'), may hold values from -6 to 6
- rope_key: bfloat16 [4, 1536, 32], P('dp', 'sp'), may hold values from -5 to 5
- latent_norm_gain: float32 [1024], replicated, may hold values from 0.1 to 1.9
- key_up_matrix: bfloat16 [2048, 1024], P('dp'), may hold values from -0.1875 to 0.1875
- value_up_matrix: bfloat16 [2048, 1024], P('dp'), may hold values from -0.1875 to 0.1875
- out_grad: bfloat16 [4, 1536, 2048], P('dp', 'sp'), may hold values from -6 to 6
Outputs:
- query_grad: bfloat16 [4, 1536, 3072], P('dp', 'sp')
- latent_grad: float32 [4, 1536, 1024], P('dp', 'sp')
- rope_key_grad: float32 [4, 1536, 32], P('dp', 'sp')
- key_weight_grad: float32 [2048, 1024], P('dp')
- value_weight_grad: float32 [2048, 1024], P('dp')
- gain_grad: float32 [1024], replicated
All inputs are finite; a program needn't handle non-finite values.
Results may differ from a plain program's by a relative error of at most 0.011.
Values may be sent and summed in bfloat16 or wider, within the bound.
A program may use at most 256 MiB of HBM per device.

v0:
```python
import jax
import jax.numpy as jnp
from jax import lax
from jax.sharding import PartitionSpec as P

ATTENTION_HEADS = 32
PLAIN_HEAD_WIDTH = 64
ROPE = 32
VALUE_HEAD_WIDTH = 64
SPAN = 64
eps = 1e-06
rope_base = 10000.0


def rotate(values, cosine, sine):
    half = values.shape[-1] // 2
    first = values[..., :half]
    second = values[..., half:]
    return jnp.concatenate(
        [first * cosine - second * sine, second * cosine + first * sine], axis=-1
    )


def angles(length, width):
    inverse = 1.0 / rope_base ** (jnp.arange(0, width, 2, dtype=jnp.float32) / width)
    turned = jnp.arange(length, dtype=jnp.float32)[:, None] * inverse[None, :]
    return (jnp.cos(turned), jnp.sin(turned))


def attend_backward(arrived, rope_full):
    f32 = jnp.float32
    bf16 = jnp.bfloat16
    length = arrived.shape[0]
    local_heads = arrived.shape[1]
    width = PLAIN_HEAD_WIDTH + ROPE
    scale = width ** (-0.5)
    block = 512
    cosine, sine = angles(length, ROPE)
    neg = jnp.finfo(f32).min
    q_nope = arrived[:, :, :PLAIN_HEAD_WIDTH]
    q_rope = rotate(
        arrived[:, :, PLAIN_HEAD_WIDTH:width].astype(f32), cosine[:, None, :], sine[:, None, :]
    ).astype(bf16)
    key_nope = arrived[:, :, width : width + PLAIN_HEAD_WIDTH]
    values = arrived[:, :, width + PLAIN_HEAD_WIDTH : width + PLAIN_HEAD_WIDTH + VALUE_HEAD_WIDTH]
    d_out = arrived[:, :, width + PLAIN_HEAD_WIDTH + VALUE_HEAD_WIDTH :]
    k_rope = rotate(rope_full.astype(f32), cosine, sine).astype(bf16)
    dk_nope = jnp.zeros((length, local_heads, PLAIN_HEAD_WIDTH), f32)
    dk_rope = jnp.zeros((length, ROPE), f32)
    d_vals = jnp.zeros((length, local_heads, VALUE_HEAD_WIDTH), f32)
    dq_parts = []
    for begin in range(0, length, block):
        end = begin + block
        qn = q_nope[begin:end]
        qr = q_rope[begin:end]
        go = d_out[begin:end]
        scores = jnp.einsum("qhd,khd->hqk", qn, key_nope[:end], preferred_element_type=f32)
        scores = (
            scores + jnp.einsum("qhd,kd->hqk", qr, k_rope[:end], preferred_element_type=f32)
        ) * scale
        q_seg = jnp.arange(begin, end) // SPAN
        k_seg = jnp.arange(end) // SPAN
        allowed = k_seg[None, :] <= q_seg[:, None]
        scores = jnp.where(allowed[None], scores, neg)
        probs = jax.nn.softmax(scores, axis=-1)
        d_probs = jnp.einsum("qhd,khd->hqk", go, values[:end], preferred_element_type=f32)
        d_scores = probs * (d_probs - jnp.sum(probs * d_probs, axis=-1, keepdims=True))
        ds_b = d_scores.astype(bf16)
        p_b = probs.astype(bf16)
        dq_n = jnp.einsum("hqk,khd->qhd", ds_b, key_nope[:end], preferred_element_type=f32) * scale
        dq_r = jnp.einsum("hqk,kd->qhd", ds_b, k_rope[:end], preferred_element_type=f32) * scale
        dq_r = rotate(dq_r, cosine[begin:end, None, :], -sine[begin:end, None, :])
        dq_parts.append(jnp.concatenate([dq_n, dq_r], axis=-1).astype(bf16))
        dk_nope = dk_nope.at[:end].add(
            jnp.einsum("hqk,qhd->khd", ds_b, qn, preferred_element_type=f32) * scale
        )
        dk_rope = dk_rope.at[:end].add(
            jnp.einsum("hqk,qhd->kd", ds_b, qr, preferred_element_type=f32) * scale
        )
        d_vals = d_vals.at[:end].add(
            jnp.einsum("hqk,qhd->khd", p_b, go, preferred_element_type=f32)
        )
    query_part = jnp.concatenate(dq_parts, axis=0)
    grads = jnp.concatenate([query_part, dk_nope.astype(bf16), d_vals.astype(bf16)], axis=-1)
    return (grads, rotate(dk_rope, cosine, -sine))


def local(query, latent, rope_key, latent_norm_gain, key_up_matrix, value_up_matrix, out_grad):
    f32 = jnp.float32
    bf16 = jnp.bfloat16
    tokens = latent.shape[1]
    width = PLAIN_HEAD_WIDTH + ROPE
    head_cols = ATTENTION_HEADS * PLAIN_HEAD_WIDTH
    lat = latent[0].astype(f32)
    inv_rms = lax.rsqrt(jnp.mean(lat * lat, axis=-1, keepdims=True) + eps)
    normed = lat * inv_rms
    nlat = (normed * latent_norm_gain).astype(bf16)
    stacked = jnp.stack([key_up_matrix, value_up_matrix])
    whole = lax.all_gather(stacked, "dp", axis=1, tiled=True)
    kv_tok = jnp.einsum("tc,gnc->tgn", nlat, whole, preferred_element_type=f32).astype(bf16)
    heads_query = query[0].reshape(tokens, ATTENTION_HEADS, width)
    key_nope = kv_tok[:, 0].reshape(tokens, ATTENTION_HEADS, PLAIN_HEAD_WIDTH)
    values = kv_tok[:, 1].reshape(tokens, ATTENTION_HEADS, VALUE_HEAD_WIDTH)
    d_out = out_grad[0].reshape(tokens, ATTENTION_HEADS, VALUE_HEAD_WIDTH)
    packed = jnp.concatenate([heads_query, key_nope, values, d_out], axis=2)
    arrived = lax.all_to_all(packed, "sp", split_axis=1, concat_axis=0, tiled=True)
    rope_full = lax.all_gather(rope_key[0], "sp", axis=0, tiled=True)
    grads_heads, rope_full_grad = attend_backward(arrived, rope_full)
    returned = lax.all_to_all(grads_heads, "sp", split_axis=0, concat_axis=1, tiled=True)
    rope_grad = lax.psum_scatter(rope_full_grad, "sp", scatter_dimension=0, tiled=True)
    query_grad = returned[:, :, :width].reshape(tokens, ATTENTION_HEADS * width)
    key_cols = returned[:, :, width : width + PLAIN_HEAD_WIDTH].reshape(tokens, head_cols)
    value_cols = returned[:, :, width + PLAIN_HEAD_WIDTH :].reshape(tokens, head_cols)
    dkv = jnp.stack([key_cols, value_cols], axis=1)
    d_nlat = jnp.einsum("tgn,gnc->tc", dkv, whole, preferred_element_type=f32)
    latents_all = lax.all_gather(nlat[None], "dp", axis=0, tiled=True)
    columns = lax.all_to_all(dkv[None], "dp", split_axis=3, concat_axis=0, tiled=True)
    partial_value = jnp.einsum("stgr,stc->grc", columns, latents_all, preferred_element_type=f32)
    weight_grads = lax.psum(partial_value, "sp")
    gain_grad = lax.psum(jnp.sum(d_nlat * normed, axis=0), ("sp", "dp"))
    scaled = d_nlat * latent_norm_gain
    latent_grad = inv_rms * (scaled - normed * jnp.mean(scaled * normed, axis=-1, keepdims=True))
    return (
        query_grad[None],
        latent_grad[None],
        rope_grad[None],
        weight_grads[0],
        weight_grads[1],
        gain_grad,
    )


def solution(mesh):
    in_specs = (
        P("dp", "sp", None),
        P("dp", "sp", None),
        P("dp", "sp", None),
        P(),
        P("dp", None),
        P("dp", None),
        P("dp", "sp", None),
    )
    out_specs = (
        P("dp", "sp", None),
        P("dp", "sp", None),
        P("dp", "sp", None),
        P("dp", None),
        P("dp", None),
        P(),
    )
    return jax.shard_map(local, mesh=mesh, in_specs=in_specs, out_specs=out_specs, check_vma=False)
```

profile of v0, /device:TPU:0, one launch (start us, length us, event | category | flops | bytes accessed | tf_op | source)
XLA Modules:
  0.0 738.0 jit_solution(6265751976223707838)
XLA Ops:
  16.4 55.1 %all-gather.4.cloned.1.call-done = bf16[2,2048,1024]{2,1,0:T(8,128)(2,1)} async-done(((bf16[2,512,1024]{2,1,0:T(8,128)(2,1)}), bf16[2,2048,1024]{2,1,0:T(8,128)(2,1)}) %all-gather.4.cloned.1.call-update) | async-done | bytes 8388624 | tf_op jit(solution)/shard_map/all_gather | solution.py:99
  71.5 6.2 convolution_convert_fusion
  87.8 5.6 pad_maximum_fusion
  97.4 5.6 all-to-all-start
  103.2 126.8 %all-gather = bf16[1,1536,32]{2,0,1:T(2,128)(2,1)S(1)} all-gather(bf16[1,192,32]{2,0,1:T(2,128)(2,1)S(1)} %copy.99), channel_id=2, replica_groups=mesh['sp'=8,'dp'=4] {'sp'}, dimensions={1}, use_global_device_ids=true | all-gather | bytes 110592 | tf_op jit(solution)/shard_map/all_gather | solution.py:107
  236.4 8.3 %copy.98 = bf16[8,192,4,288]{1,0,3,2:T(8,128)(2,1)} copy(bf16[8,192,4,288]{3,1,2,0:T(8,128)(2,1)} %bitcast.8) | data formatting | bytes 7077888 | tf_op jit(solution)/shard_map/all_to_all | solution.py:106
  244.7 6.9 all_to_all.42
  283.7 9.7 %multiply_convert_fusion.1 = bf16[4,512,1024]{2,1,0:T(8,128)(2,1)S(1)} fusion(f32[4,512,1024]{2,1,0:T(8,128)S(1)} %get-tuple-element.177, f32[4,512]{1,0:T(4,128)S(1)} %get-tuple-element.176, f32[4,512,1024]{2,1,0:T(8,128)S(1)} %get-tuple-element.171, f32[4,512]{1,0:T(4,128)S(1)} %get-tuple-element.170), kind=kLoop, calls=%fused_computation.12 | loop fusion | flops 8388608 | bytes 20987904 | tf_op jit(solution)/shard_map/convert_element_type | solution.py:68
  300.5 8.5 %fusion.4 = f32[4,512,1536]{2,1,0:T(8,128)} fusion(f32[1536,512,4]{0,1,2:T(8,128)S(1)} %fusion.114, pred[512,1536]{1,0:T(8,128)(4,1)S(1)} %copy-done.13, bf16[1536,4,288]{0,2,1:T(8,128)(2,1)} %copy-done.3), kind=kOutput, calls=%fused_computation.5 | convolution fusion | flops 412090368 | bytes 27000832 | tf_op jit(solution)/shard_map/qhd,khd->hqk/dot_general | solution.py:57
  309.1 14.9 %fusion.154 = (f32[4,512]{1,0:T(4,128)S(1)}, f32[4,512,1536]{2,1,0:T(8,128)}) fusion(f32[4,512,1536]{2,1,0:T(8,128)} %fusion.4), kind=kOutput, calls=%fused_computation.226 | output fusion | flops 6292991 | bytes 25174016 | tf_op jit(solution)/shard_map/sub | solution.py:65
  323.9 11.8 %multiply_reduce_fusion = (f32[4,512]{1,0:T(4,128)S(1)}, f32[4,512,1536]{2,1,0:T(8,128)}) fusion(f32[4,512,1536]{2,1,0:T(8,128)} %get-tuple-element.173, f32[4,512]{1,0:T(4,128)S(1)} %get-tuple-element.172, bf16[1536,4,288]{0,2,1:T(8,128)(2,1)} %copy-done.3), kind=kOutput, calls=%fused_computation.7 | convolution fusion | flops 412088320 | bytes 26230784 | tf_op jit(solution)/shard_map/qhd,khd->hqk/dot_general | solution.py:66
  335.7 6.0 multiply_convert_fusion
  351.6 11.2 %fusion.37 = f32[1536,4,64]{0,2,1:T(8,128)} fusion(f32[1536,4,64]{0,2,1:T(8,128)} %scatter-add.24, bf16[1536,4,288]{0,2,1:T(8,128)(2,1)} %copy-done.3, f32[4,512]{1,0:T(4,128)S(1)} %get-tuple-element.170, f32[4,512,1024]{2,1,0:T(8,128)} %copy-done.2), kind=kOutput, calls=%fused_computation.53 | convolution fusion | flops 274992128 | bytes 19144704 | tf_op jit(solution)/shard_map/hqk,qhd->khd/dot_general | solution.py:81
  367.2 13.7 %fusion.22 = bf16[1536,4,64]{0,2,1:T(8,128)(2,1)} fusion(f32[1536,4,64]{0,2,1:T(8,128)} %fusion.37, bf16[1536,4,288]{0,2,1:T(8,128)(2,1)} %copy-done.3, f32[4,512]{1,0:T(4,128)S(1)} %get-tuple-element.172, f32[4,512,1536]{2,1,0:T(8,128)} %fusion.4), kind=kOutput, calls=%fused_computation.36 | convolution fusion | flops 412880384 | bytes 27795456 | tf_op jit(solution)/shard_map/hqk,qhd->khd/dot_general | solution.py:81
  388.8 5.8 copy.107
  401.9 64.4 %all-to-all-done.1 = bf16[1536,4,224]{2,1,0:T(4,128)(2,1)} async-done(((bf16[1536,4,224]{2,1,0:T(4,128)(2,1)}), bf16[1536,4,224]{2,1,0:T(4,128)(2,1)}, u32[]{:S(2)}, u32[]{:S(2)}) %all-to-all-start.1) | async-done | bytes 2752544 | tf_op jit(solution)/shard_map/all_to_all | solution.py:109
  483.8 6.1 copy.116
  503.7 16.3 %all-to-all-done.2 = bf16[1,192,2,2048]{1,2,0,3:T(2,128)(2,1)} async-done(((bf16[1,192,2,2048]{1,2,0,3:T(2,128)(2,1)}), bf16[1,192,2,2048]{1,2,0,3:T(2,128)(2,1)}, u32[]{:S(2)}, u32[]{:S(2)}) %all-to-all-start.2) | async-done | bytes 1572896 | tf_op jit(solution)/shard_map/all_to_all | solution.py:117
  520.0 6.0 copy.118
  526.0 5.7 convolution_bitcast_fusion.1
  531.7 34.6 %reduce-scatter.4.cloned.1.call-done = f32[192,32]{1,0:T(8,128)} async-done(((f32[1536,32]{1,0:T(8,128)}), f32[192,32]{1,0:T(8,128)}) %reduce-scatter.4.cloned.1.call-update) | async-done | bytes 24592
  572.2 6.3 fusion.72
  578.5 44.0 %psum.15 = f32[1024]{0:T(1024)} all-reduce(f32[1024]{0:T(1024)S(1)} %get-tuple-element.138), channel_id=1, replica_groups=mesh['sp'=8,'dp'=4] {'sp','dp'}, use_global_device_ids=true, to_apply=%region_14.15 | all-reduce | flops 1024 | bytes 8192 | tf_op jit(solution)/shard_map/psum | solution.py:120
  623.6 102.6 %all-reduce.5.cloned.1.call-done = f32[2,512,1024]{2,1,0:T(8,128)} async-done(((f32[2,512,1024]{2,1,0:T(8,128)}), f32[2,512,1024]{2,1,0:T(8,128)}) %all-reduce.5.cloned.1.call-update) | async-done | bytes 4194320 | tf_op jit(solution)/shard_map/psum | solution.py:119
  (192 shorter events, 140.9 us)
Async XLA Ops:
  7.2 64.3 %all-gather.4.cloned.1.call-start = ((), (), s32[]{:S(2)}) async-start(), calls=%async_computation.4 | async-start | bytes 10485760 | tf_op jit(solution)/shard_map/all_gather | solution.py:99
  10.3 5.9 copy-start.10
  10.4 61.1 %copy-start.41 = (f32[1024]{0:T(1024)S(1)}, f32[1024]{0:T(1024)}, u32[]{:S(2)}) copy-start(f32[1024]{0:T(1024)} %param.34) | copy-start | bytes 12292
  16.4 55.1 %copy-start.44 = (f32[192]{0:T(256)}, f32[192]{0:T(256)S(1)}, u32[]{:S(2)}) copy-start(f32[192]{0:T(256)S(1)} %add_rsqrt_fusion) | copy-start | bytes 2308
  97.4 5.7 copy-start.43
  97.4 139.0 %all-to-all-start = ((bf16[192,32,288]{2,0,1:T(8,128)(2,1)}), bf16[192,32,288]{2,0,1:T(8,128)(2,1)}, u32[]{:S(2)}, u32[]{:S(2)}) async-start(bf16[192,32,288]{2,0,1:T(8,128)(2,1)} %copy.97), calls=%async_computation | async-start | bytes 9437184 | tf_op jit(solution)/shard_map/all_to_all | solution.py:106
  251.6 11.8 %copy-start.3 = (bf16[1536,4,288]{0,2,1:T(8,128)(2,1)}, bf16[1536,4,288]{0,2,1:T(8,128)(2,1)S(1)}, u32[]{:S(2)}) copy-start(bf16[1536,4,288]{0,2,1:T(8,128)(2,1)S(1)} %all_to_all.42) | copy-start | bytes 10616836
  268.0 5.0 copy-start.7
  268.0 5.0 copy-start.9
  293.4 5.2 copy-start.1
  323.9 11.8 %slice-start = ((s8[12582912]{0:T(1024)(128)(4,1)}), s8[4194304]{0:T(1024)(128)(4,1)S(1)}, s32[]{:S(2)}) async-start(s8[12582912]{0:T(1024)(128)(4,1)} %bitcast.187), calls=%async_computation.8 | async-start | bytes 8388608
  323.9 11.8 %slice-start.1 = ((s8[12582912]{0:T(1024)(128)(4,1)}), s8[4194304]{0:T(1024)(128)(4,1)S(1)}, s32[]{:S(2)}) async-start(s8[12582912]{0:T(1024)(128)(4,1)} %bitcast.187), calls=%async_computation.9 | async-start | bytes 8388608
  323.9 11.8 %slice-start.2 = ((s8[12582912]{0:T(1024)(128)(4,1)}), s8[4194304]{0:T(1024)(128)(4,1)S(1)}, s32[]{:S(2)}) async-start(s8[12582912]{0:T(1024)(128)(4,1)} %bitcast.187), calls=%async_computation.10 | async-start | bytes 8388608
  341.8 7.1 copy-start
  380.9 4.9 copy-start.25
  381.0 4.9 copy-start.26
  381.0 4.9 copy-start.27
  381.0 4.9 copy-start.33
  394.6 4.9 copy-start.45
  394.6 71.6 %all-to-all-start.1 = ((bf16[1536,4,224]{2,1,0:T(4,128)(2,1)}), bf16[1536,4,224]{2,1,0:T(4,128)(2,1)}, u32[]{:S(2)}, u32[]{:S(2)}) async-start(bf16[1536,4,224]{2,1,0:T(4,128)(2,1)} %copy.107), calls=%async_computation.1 | async-start | bytes 6291456 | tf_op jit(solution)/shard_map/all_to_all | solution.py:109
  399.2 126.8 %all-gather.6.cloned.1.call-start = ((), (), s32[]{:S(2)}) async-start(), calls=%async_computation.5 | async-start | bytes 1966080 | tf_op jit(solution)/shard_map/all_gather | solution.py:116
  489.8 30.2 %all-to-all-start.2 = ((bf16[1,192,2,2048]{1,2,0,3:T(2,128)(2,1)}), bf16[1,192,2,2048]{1,2,0,3:T(2,128)(2,1)}, u32[]{:S(2)}, u32[]{:S(2)}) async-start(bf16[1,192,2,2048]{1,2,0,3:T(2,128)(2,1)} %copy.116), calls=%async_computation.2 | async-start | bytes 4194304 | tf_op jit(solution)/shard_map/all_to_all | solution.py:117
  494.3 72.0 %reduce-scatter.4.cloned.1.call-start = ((), (), s32[]{:S(2)}) async-start(), calls=%async_computation.7 | async-start | bytes 884736
  503.6 222.6 %all-reduce.5.cloned.1.call-start = ((), (), s32[]{:S(2)}) async-start(), calls=%async_computation.6 | async-start | bytes 8388608 | tf_op jit(solution)/shard_map/psum | solution.py:119
  (34 other events, 102.9 us)
Sparse Core Ops, SparseCore 0:
  10.5 60.9 all-gather.3
  401.6 19.9 all-gather.5
  503.8 62.4 reduce-scatter.3
  569.8 156.3 all-reduce.4
where the time goes:
time: 747 us; the launch traced here: 738 us
  waiting for transfers between devices  273 us (37%)
  blocking collectives  171 us (23%)
  matrix products  118 us (16%)
  local copies, waits for them, and re-layouts  87 us (12%)
  other arithmetic  59.6 us (8%)
  starting transfers between devices  15.1 us (2%)
  between operations  15 us (2%)
    all_gather x1, blocking collectives, local(): rope_full = lax.all_gather(rope_key[0], 'sp', axis=0, tiled=True)  127 us
    psum x1, waiting for transfers between devices, local(): weight_grads = lax.psum(partial_value, 'sp')  103 us
    all_to_all x1, waiting for transfers between devices, local(): lax.all_to_all(grads_heads, 'sp', split_axis=0, concat_axis=1, tiled=True)  64.4 us
    all_gather x1, waiting for transfers between devices, local(): whole = lax.all_gather(stacked, 'dp', axis=1, tiled=True)  55.1 us
    psum x1, blocking collectives, local(): gain_grad = lax.psum(jnp.sum(d_nlat * normed, axis=0), ('sp', 'dp'))  44 us
    unnamed x5, waiting for transfers between devices  34.6 us
    dot_general x3, matrix products, attend_backward(): jnp.einsum('hqk,qhd->khd', p_b, go, preferred_element_type=f32)  30.3 us
    sub x3, other arithmetic, attend_backward(): probs = jax.nn.softmax(scores, axis=-1)  20.1 us
  transfers between devices with their start and end apart: 7, of which 5 were waited for; matrix products, arithmetic and copies ran while one was open for 10% of the time, Pallas kernels for 0%

commit v1 on v0

--- a/solution.py
+++ b/solution.py
@@ -96,7 +96,7 @@
     normed = lat * inv_rms
     nlat = (normed * latent_norm_gain).astype(bf16)
     stacked = jnp.stack([key_up_matrix, value_up_matrix])
-    whole = lax.all_gather(stacked, "dp", axis=1, tiled=True)
+    whole = jnp.concatenate(lax.all_gather(stacked, "dp"), axis=1)
     kv_tok = jnp.einsum("tc,gnc->tgn", nlat, whole, preferred_element_type=f32).astype(bf16)
     heads_query = query[0].reshape(tokens, ATTENTION_HEADS, width)
     key_nope = kv_tok[:, 0].reshape(tokens, ATTENTION_HEADS, PLAIN_HEAD_WIDTH)

time: 747 us -> 748 us (level)
  other arithmetic: 59.6 us -> 50.7 us
  local copies, waits for them, and re-layouts: 87 us -> 94.5 us
    convert_element_type x3, other arithmetic: 17 us -> 8.81 us  [attend_backward(): ds_b = d_scores.astype(bf16)]
    all_gather x0 -> x1, local copies, waits for them, and re-layouts: none -> 7.57 us  [local(): whole = jnp.concatenate(lax.all_gather(stacked, 'dp'), axis=1)]
where the time goes in v1:
time: 748 us; the launch traced here: 737 us
  waiting for transfers between devices  274 us (37%)
  blocking collectives  171 us (23%)
  matrix products  118 us (16%)
  local copies, waits for them, and re-layouts  94.5 us (13%)
  other arithmetic  50.7 us (7%)
  between operations  15 us (2%)
  starting transfers between devices  14.9 us (2%)
    all_gather x1, blocking collectives, local(): rope_full = lax.all_gather(rope_key[0], 'sp', axis=0, tiled=True)  127 us
    psum x1, waiting for transfers between devices, local(): weight_grads = lax.psum(partial_value, 'sp')  103 us
    all_to_all x1, waiting for transfers between devices, local(): lax.all_to_all(grads_heads, 'sp', split_axis=0, concat_axis=1, tiled=True)  64.9 us
    all_gather x1, waiting for transfers between devices, local(): whole = jnp.concatenate(lax.all_gather(stacked, 'dp'), axis=1)  54.9 us
    psum x1, blocking collectives, local(): gain_grad = lax.psum(jnp.sum(d_nlat * normed, axis=0), ('sp', 'dp'))  44 us
    unnamed x5, waiting for transfers between devices  35.1 us
    dot_general x3, matrix products, attend_backward(): jnp.einsum('hqk,qhd->khd', p_b, go, preferred_element_type=f32)  30.3 us
    sub x3, other arithmetic, attend_backward(): probs = jax.nn.softmax(scores, axis=-1)  20.1 us
  transfers between devices with their start and end apart: 7, of which 5 were waited for; matrix products, arithmetic and copies ran while one was open for 10% of the time, Pallas kernels for 0%

profile of v1, /device:TPU:0, one launch (start us, length us, event | category | flops | bytes accessed | tf_op | source)
XLA Modules:
  0.0 737.4 jit_solution(639299617381466546)
XLA Ops:
  16.6 54.9 %all-gather.7.cloned.1.call-done = bf16[8,512,1024]{2,1,0:T(8,128)(2,1)} async-done(((bf16[2,512,1024]{2,1,0:T(8,128)(2,1)}), bf16[8,512,1024]{2,1,0:T(8,128)(2,1)}) %all-gather.7.cloned.1.call-update) | async-done | bytes 8388624 | tf_op jit(solution)/shard_map/all_gather | solution.py:99
  71.5 7.6 %copy.95 = bf16[4,2,512,1024]{3,2,0,1:T(8,128)(2,1)} copy(bf16[4,2,512,1024]{3,2,1,0:T(8,128)(2,1)} %bitcast.192) | data formatting | bytes 16777216 | tf_op jit(solution)/shard_map/all_gather | solution.py:99
  79.1 6.3 convolution_convert_fusion
  95.4 5.6 pad_maximum_fusion
  105.0 5.6 all-to-all-start
  110.8 126.8 %all-gather.1 = bf16[1,1536,32]{2,0,1:T(2,128)(2,1)S(1)} all-gather(bf16[1,192,32]{2,0,1:T(2,128)(2,1)S(1)} %copy.104), channel_id=3, replica_groups=mesh['sp'=8,'dp'=4] {'sp'}, dimensions={1}, use_global_device_ids=true | all-gather | bytes 110592 | tf_op jit(solution)/shard_map/all_gather | solution.py:107
  244.0 8.3 %copy.103 = bf16[8,192,4,288]{1,0,3,2:T(8,128)(2,1)} copy(bf16[8,192,4,288]{3,1,2,0:T(8,128)(2,1)} %bitcast.12) | data formatting | bytes 7077888 | tf_op jit(solution)/shard_map/all_to_all | solution.py:106
  252.4 6.9 all_to_all.42
  300.0 8.5 %fusion.4 = f32[4,512,1536]{2,1,0:T(8,128)} fusion(f32[1536,512,4]{0,1,2:T(8,128)S(1)} %fusion.109, pred[512,1536]{1,0:T(8,128)(4,1)S(1)} %copy-done.12, bf16[1536,4,288]{0,2,1:T(8,128)(2,1)} %copy-done.3), kind=kOutput, calls=%fused_computation.5 | convolution fusion | flops 412090368 | bytes 27000832 | tf_op jit(solution)/shard_map/qhd,khd->hqk/dot_general | solution.py:57
  308.5 14.9 %fusion.149 = (f32[4,512]{1,0:T(4,128)S(1)}, f32[4,512,1536]{2,1,0:T(8,128)}) fusion(f32[4,512,1536]{2,1,0:T(8,128)} %fusion.4), kind=kOutput, calls=%fused_computation.222 | output fusion | flops 6292991 | bytes 25174016 | tf_op jit(solution)/shard_map/sub | solution.py:65
  323.4 11.8 %multiply_reduce_fusion = (f32[4,512]{1,0:T(4,128)S(1)}, f32[4,512,1536]{2,1,0:T(8,128)}) fusion(f32[4,512,1536]{2,1,0:T(8,128)} %get-tuple-element.173, f32[4,512]{1,0:T(4,128)S(1)} %get-tuple-element.172, bf16[1536,4,288]{0,2,1:T(8,128)(2,1)} %copy-done.3), kind=kOutput, calls=%fused_computation.7 | convolution fusion | flops 412088320 | bytes 26230784 | tf_op jit(solution)/shard_map/qhd,khd->hqk/dot_general | solution.py:66
  335.2 6.0 multiply_convert_fusion
  351.1 11.2 %fusion.37 = f32[1536,4,64]{0,2,1:T(8,128)} fusion(f32[1536,4,64]{0,2,1:T(8,128)} %scatter-add.24, bf16[1536,4,288]{0,2,1:T(8,128)(2,1)} %copy-done.3, f32[4,512]{1,0:T(4,128)S(1)} %get-tuple-element.170, f32[4,512,1024]{2,1,0:T(8,128)} %copy-done.2), kind=kOutput, calls=%fused_computation.53 | convolution fusion | flops 274992128 | bytes 19144704 | tf_op jit(solution)/shard_map/hqk,qhd->khd/dot_general | solution.py:81
  366.6 13.7 %fusion.22 = bf16[1536,4,64]{0,2,1:T(8,128)(2,1)} fusion(f32[1536,4,64]{0,2,1:T(8,128)} %fusion.37, bf16[1536,4,288]{0,2,1:T(8,128)(2,1)} %copy-done.3, f32[4,512]{1,0:T(4,128)S(1)} %get-tuple-element.172, f32[4,512,1536]{2,1,0:T(8,128)} %fusion.4), kind=kOutput, calls=%fused_computation.36 | convolution fusion | flops 412880384 | bytes 27795456 | tf_op jit(solution)/shard_map/hqk,qhd->khd/dot_general | solution.py:81
  388.3 5.8 copy.112
  400.7 64.9 %all-to-all-done.1 = bf16[1536,4,224]{2,1,0:T(4,128)(2,1)} async-done(((bf16[1536,4,224]{2,1,0:T(4,128)(2,1)}), bf16[1536,4,224]{2,1,0:T(4,128)(2,1)}, u32[]{:S(2)}, u32[]{:S(2)}) %all-to-all-start.1) | async-done | bytes 2752544 | tf_op jit(solution)/shard_map/all_to_all | solution.py:109
  483.1 6.1 copy.121
  503.0 16.3 %all-to-all-done.2 = bf16[1,192,2,2048]{1,2,0,3:T(2,128)(2,1)} async-done(((bf16[1,192,2,2048]{1,2,0,3:T(2,128)(2,1)}), bf16[1,192,2,2048]{1,2,0,3:T(2,128)(2,1)}, u32[]{:S(2)}, u32[]{:S(2)}) %all-to-all-start.2) | async-done | bytes 1572896 | tf_op jit(solution)/shard_map/all_to_all | solution.py:117
  519.3 6.0 copy.123
  525.3 5.7 convolution_bitcast_fusion.1
  531.1 34.6 %reduce-scatter.4.cloned.1.call-done = f32[192,32]{1,0:T(8,128)} async-done(((f32[1536,32]{1,0:T(8,128)}), f32[192,32]{1,0:T(8,128)}) %reduce-scatter.4.cloned.1.call-update) | async-done | bytes 24592
  571.6 6.3 fusion.70
  577.9 44.0 %psum.15 = f32[1024]{0:T(1024)} all-reduce(f32[1024]{0:T(1024)S(1)} %get-tuple-element.138), channel_id=1, replica_groups=mesh['sp'=8,'dp'=4] {'sp','dp'}, use_global_device_ids=true, to_apply=%region_14.15 | all-reduce | flops 1024 | bytes 8192 | tf_op jit(solution)/shard_map/psum | solution.py:120
  623.0 102.6 %all-reduce.5.cloned.1.call-done = f32[2,512,1024]{2,1,0:T(8,128)} async-done(((f32[2,512,1024]{2,1,0:T(8,128)}), f32[2,512,1024]{2,1,0:T(8,128)}) %all-reduce.5.cloned.1.call-update) | async-done | bytes 4194320 | tf_op jit(solution)/shard_map/psum | solution.py:119
  (193 shorter events, 142.0 us)
Async XLA Ops:
  7.2 64.3 %all-gather.7.cloned.1.call-start = ((), (), s32[]{:S(2)}) async-start(), calls=%async_computation.6 | async-start | bytes 10485760 | tf_op jit(solution)/shard_map/all_gather | solution.py:99
  10.3 5.9 copy-start.10
  10.4 6.0 copy-start.41
  16.4 62.7 %copy-start.44 = (f32[192]{0:T(256)}, f32[192]{0:T(256)S(1)}, u32[]{:S(2)}) copy-start(f32[192]{0:T(256)S(1)} %add_rsqrt_fusion) | copy-start | bytes 2308
  16.6 62.5 %copy-start.20 = (bf16[1,192,1024]{2,1,0:T(8,128)(2,1)}, bf16[1,192,1024]{2,1,0:T(8,128)(2,1)S(1)}, u32[]{:S(2)}) copy-start(bf16[1,192,1024]{2,1,0:T(8,128)(2,1)S(1)} %fusion.73) | copy-start | bytes 1179652
  105.0 5.7 copy-start.43
  105.0 139.0 %all-to-all-start = ((bf16[192,32,288]{2,0,1:T(8,128)(2,1)}), bf16[192,32,288]{2,0,1:T(8,128)(2,1)}, u32[]{:S(2)}, u32[]{:S(2)}) async-start(bf16[192,32,288]{2,0,1:T(8,128)(2,1)} %copy.102), calls=%async_computation | async-start | bytes 9437184 | tf_op jit(solution)/shard_map/all_to_all | solution.py:106
  259.2 11.8 %copy-start.3 = (bf16[1536,4,288]{0,2,1:T(8,128)(2,1)}, bf16[1536,4,288]{0,2,1:T(8,128)(2,1)S(1)}, u32[]{:S(2)}) copy-start(bf16[1536,4,288]{0,2,1:T(8,128)(2,1)S(1)} %all_to_all.42) | copy-start | bytes 10616836
  275.6 5.0 copy-start.7
  275.7 5.0 copy-start.9
  292.9 5.2 copy-start.1
  323.4 11.8 %slice-start = ((s8[12582912]{0:T(1024)(128)(4,1)}), s8[4194304]{0:T(1024)(128)(4,1)S(1)}, s32[]{:S(2)}) async-start(s8[12582912]{0:T(1024)(128)(4,1)} %bitcast.185), calls=%async_computation.8 | async-start | bytes 8388608
  323.4 11.8 %slice-start.1 = ((s8[12582912]{0:T(1024)(128)(4,1)}), s8[4194304]{0:T(1024)(128)(4,1)S(1)}, s32[]{:S(2)}) async-start(s8[12582912]{0:T(1024)(128)(4,1)} %bitcast.185), calls=%async_computation.9 | async-start | bytes 8388608
  323.4 11.8 %slice-start.2 = ((s8[12582912]{0:T(1024)(128)(4,1)}), s8[4194304]{0:T(1024)(128)(4,1)S(1)}, s32[]{:S(2)}) async-start(s8[12582912]{0:T(1024)(128)(4,1)} %bitcast.185), calls=%async_computation.10 | async-start | bytes 8388608
  341.3 7.1 copy-start
  380.4 4.9 copy-start.25
  380.4 4.9 copy-start.26
  380.4 4.9 copy-start.27
  380.4 4.9 copy-start.33
  394.1 71.5 %all-to-all-start.1 = ((bf16[1536,4,224]{2,1,0:T(4,128)(2,1)}), bf16[1536,4,224]{2,1,0:T(4,128)(2,1)}, u32[]{:S(2)}, u32[]{:S(2)}) async-start(bf16[1536,4,224]{2,1,0:T(4,128)(2,1)} %copy.112), calls=%async_computation.1 | async-start | bytes 6291456 | tf_op jit(solution)/shard_map/all_to_all | solution.py:109
  398.5 126.8 %all-gather.5.cloned.1.call-start = ((), (), s32[]{:S(2)}) async-start(), calls=%async_computation.4 | async-start | bytes 1966080 | tf_op jit(solution)/shard_map/all_gather | solution.py:116
  489.1 30.2 %all-to-all-start.2 = ((bf16[1,192,2,2048]{1,2,0,3:T(2,128)(2,1)}), bf16[1,192,2,2048]{1,2,0,3:T(2,128)(2,1)}, u32[]{:S(2)}, u32[]{:S(2)}) async-start(bf16[1,192,2,2048]{1,2,0,3:T(2,128)(2,1)} %copy.121), calls=%async_computation.2 | async-start | bytes 4194304 | tf_op jit(solution)/shard_map/all_to_all | solution.py:117
  493.6 72.1 %reduce-scatter.4.cloned.1.call-start = ((), (), s32[]{:S(2)}) async-start(), calls=%async_computation.7 | async-start | bytes 884736
  503.0 222.7 %all-reduce.5.cloned.1.call-start = ((), (), s32[]{:S(2)}) async-start(), calls=%async_computation.5 | async-start | bytes 8388608 | tf_op jit(solution)/shard_map/psum | solution.py:119
  (34 other events, 101.7 us)
Sparse Core Ops, SparseCore 0:
  10.5 60.9 all-gather.6
  400.9 19.9 all-gather.4
  503.1 62.5 reduce-scatter.3
  569.2 156.3 all-reduce.4
